TPU v7x, 32 devices: a whole 2x2x4 slice. The times are simulated.
32 devices in a mesh: kv: 8 (over z, y), tp: 4 (over x, core).
Axes of the slice: x: 2, y: 2, z: 4, core: 2. Of those that a mesh axis runs over, the one named last changes fastest.
Arguments:
- tokens: bfloat16 [16, 4096], P(None, 'kv')
- norm_gain: float32 [4096], P('kv'), may hold values from 0.1 to 1.9
- w_query: bfloat16 [4096, 3072], P('kv', 'tp'), may hold values from -0.09375 to 0.09375
- w_key: bfloat16 [4096, 3072], P('kv', 'tp'), may hold values from -0.09375 to 0.09375
- w_value: bfloat16 [4096, 3072], P('kv', 'tp'), may hold values from -0.09375 to 0.09375
- w_forget: bfloat16 [4096, 48], P('kv'), may hold values from -0.09375 to 0.09375
- w_out: bfloat16 [3072, 4096], P('tp', 'kv'), may hold values from -0.109375 to 0.109375
- mix_gain: float32 [4096], P('kv'), may hold values from 0.1 to 1.9
- w_up: bfloat16 [4096, 16384], P('kv', 'tp'), may hold values from -0.09375 to 0.09375
- w_down: bfloat16 [16384, 4096], P('tp', 'kv'), may hold values from -0.0625 to 0.0625
- key_cache: bfloat16 [16, 1024, 3072], P(None, 'kv', 'tp')
- value_cache: bfloat16 [16, 1024, 3072], P(None, 'kv', 'tp'), may hold values from -6 to 6
- decay_cache: float32 [16, 48, 1024], P(None, 'tp', 'kv')
- lengths: int32 [16], replicated, may hold values from 1 to 1024, 5461 in all
Outputs:
- layer_out: bfloat16 [16, 4096], P(None, 'kv')
Inputs may be any that keep to these rules, and one draw needn't show every extreme that they name: `lengths`: one sequence fills all 1024 positions.
All inputs are finite; a program needn't handle non-finite values.
Results may differ from a plain program's by a relative error of at most 0.01.
Values may be sent and summed in bfloat16 or wider, within the bound.
A program may use at most 64 MiB of HBM per device.

v0:
```python
import jax
import jax.numpy as jnp
from jax import lax
from jax.sharding import PartitionSpec as P

HEAD_DIM = 64


epsilon = 1e-06
very_low = -1e30


def local_softmax(query_heads, score_bias, keys_block, values_block, live_mask):
    rows_count, count = (keys_block.shape[0], keys_block.shape[1])
    heads_count = query_heads.shape[1]
    keys_view = keys_block.reshape(rows_count, count, heads_count, HEAD_DIM)
    values_view = values_block.reshape(rows_count, count, heads_count, HEAD_DIM)
    scores = jnp.einsum("bhe,bphe->bhp", query_heads, keys_view, preferred_element_type=jnp.float32)
    scores = scores * HEAD_DIM ** (-0.5) + score_bias
    block_peak = jnp.max(jnp.where(live_mask, scores, very_low), axis=2)
    weights = jnp.where(live_mask, jnp.exp(scores - block_peak[..., None]), 0.0)
    totals = jnp.sum(weights, axis=2)
    weighted = jnp.einsum(
        "bhp,bphe->bhe",
        weights.astype(jnp.bfloat16),
        values_view,
        preferred_element_type=jnp.float32,
    )
    return (block_peak, totals, weighted)


def shards(
    tokens,
    norm_gain,
    w_query,
    w_key,
    w_value,
    w_forget,
    w_out,
    mix_gain,
    w_up,
    w_down,
    key_cache,
    value_cache,
    decay_cache,
    lengths,
):
    rows_count = tokens.shape[0]
    width = tokens.shape[1] * lax.axis_size("kv")
    heads_here = decay_cache.shape[1]
    span = key_cache.shape[1]
    tokens_f = tokens.astype(jnp.float32)
    scaled_in = (tokens_f * norm_gain).astype(jnp.bfloat16)
    forget_cols = lax.dynamic_slice_in_dim(
        w_forget, lax.axis_index("tp") * heads_here, heads_here, 1
    )
    positions = lax.axis_index("kv") * span + jnp.arange(span, dtype=jnp.int32)
    newest = positions[None, None, :] == (lengths - 1)[:, None, None]
    summed = lax.psum(
        (
            jnp.dot(scaled_in, w_query, preferred_element_type=jnp.float32),
            jnp.dot(scaled_in, w_key, preferred_element_type=jnp.float32),
            jnp.dot(scaled_in, w_value, preferred_element_type=jnp.float32),
            jnp.dot(scaled_in, forget_cols, preferred_element_type=jnp.float32),
            jnp.sum(tokens_f * tokens_f, axis=1),
            jnp.sum(jnp.where(newest, decay_cache, 0.0), axis=2),
        ),
        "kv",
    )
    row_scale = lax.rsqrt(summed[4] / width + epsilon)[:, None]
    queries = (row_scale * summed[0]).astype(jnp.bfloat16)
    new_keys = (row_scale * summed[1]).astype(jnp.bfloat16)
    new_values = (row_scale * summed[2]).astype(jnp.bfloat16)
    now_decay = summed[5] + jax.nn.log_sigmoid(row_scale * summed[3])
    query_heads = queries.reshape(rows_count, heads_here, HEAD_DIM)
    own_score = jnp.sum(
        query_heads.astype(jnp.float32)
        * new_keys.astype(jnp.float32).reshape(rows_count, heads_here, HEAD_DIM),
        axis=2,
    ) * HEAD_DIM ** (-0.5)
    own_values = new_values.astype(jnp.float32).reshape(rows_count, heads_here, HEAD_DIM)
    live_mask = positions[None, None, :] < lengths[:, None, None]
    local_state = local_softmax(
        query_heads, now_decay[:, :, None] - decay_cache, key_cache, value_cache, live_mask
    )
    global_peak = lax.pmax(local_state[0], "kv")
    highest = jnp.maximum(global_peak, own_score)
    factor_here = jnp.exp(local_state[0] - highest)
    total_sum, weighted_sum = lax.psum(
        (local_state[1] * factor_here, local_state[2] * factor_here[..., None]), "kv"
    )
    factor_own = jnp.exp(own_score - highest)
    final_state = (
        highest,
        total_sum + factor_own,
        weighted_sum + factor_own[..., None] * own_values,
    )
    attended = (
        (final_state[2] / final_state[1][..., None])
        .reshape(rows_count, heads_here * HEAD_DIM)
        .astype(jnp.bfloat16)
    )
    head_terms = lax.psum(jnp.dot(attended, w_out, preferred_element_type=jnp.float32), "tp")
    mixed_f = (tokens_f + head_terms).astype(jnp.bfloat16).astype(jnp.float32)
    mix_in = (mixed_f * mix_gain).astype(jnp.bfloat16)
    up_terms = jnp.dot(mix_in, w_up, preferred_element_type=jnp.float32)
    squares_here = jnp.sum(mixed_f * mixed_f, axis=1)
    upward, squares_all = lax.psum((up_terms, squares_here), "kv")
    mix_scale = lax.rsqrt(squares_all / width + epsilon)[:, None]
    hidden = (jax.nn.relu(mix_scale * upward) ** 2).astype(jnp.bfloat16)
    down_terms = jnp.dot(hidden, w_down, preferred_element_type=jnp.float32)
    channel_terms = lax.psum(down_terms, "tp")
    return (mixed_f + channel_terms).astype(jnp.bfloat16)


def solution(mesh):
    placed = (
        P(None, "kv"),
        P("kv"),
        P("kv", "tp"),
        P("kv", "tp"),
        P("kv", "tp"),
        P("kv", None),
        P("tp", "kv"),
        P("kv"),
        P("kv", "tp"),
        P("tp", "kv"),
        P(None, "kv", "tp"),
        P(None, "kv", "tp"),
        P(None, "tp", "kv"),
        P(),
    )
    return jax.shard_map(
        shards, mesh=mesh, in_specs=placed, out_specs=P(None, "kv"), check_vma=False
    )
```

profile of v0, /device:TPU:0, one launch (start us, length us, event | category | flops | bytes accessed | tf_op | source)
XLA Modules:
  0.0 298.8 jit_solution(791732732799819180)
XLA Ops:
  6.5 0.7 broadcast_add_fusion
  7.3 1.4 fusion.9
  8.6 0.7 broadcast_compare_fusion
  9.4 1.0 select_reduce_fusion.1
  10.4 0.7 copy.31
  11.1 1.6 fusion.29
  12.6 2.0 fusion.26
  14.6 1.5 fusion.20
  16.1 0.0 all-reduce.8.cloned.1.call-start
  16.2 2.0 fusion.24
  18.2 4.7 %copy.30 = bf16[16,128,768]{1,2,0:T(8,128)(2,1)} copy(bf16[16,128,768]{2,1,0:T(8,128)(2,1)} %param.24) | data formatting | bytes 6291456 | tf_op args[10]
  22.9 4.6 %copy.33 = bf16[16,128,768]{1,2,0:T(8,128)(2,1)} copy(bf16[16,128,768]{2,1,0:T(8,128)(2,1)} %param.25) | data formatting | bytes 6291456 | tf_op args[11]
  27.5 62.4 %all-reduce.10.cloned.1.call-done = (f32[16,768]{1,0:T(8,128)}, f32[16]{0:T(128)}, f32[16,12]{1,0:T(8,128)}, f32[16,12]{1,0:T(8,128)}, f32[16,768]{1,0:T(8,128)}) async-done(((f32[16,768]{1,0:T(8,128)}, f32[16]{0:T(128)}, f32[16,12]{1,0:T(8,128)}, f32[16,12]{1,0:T(8,128)}, f32[16,768]{1,0:T(8,128)}), (f32[16,768]{1,0:T(8,128)}, f32[16]{0:T(128)}, f32[16,12]{1,0:T(8,128)}, f32[16,12]{1,0:T(8,128)}, ...) | async-done | bytes 99920 | tf_op jit(solution)/shard_map/psum | solution.py:59
  89.9 0.6 add_rsqrt_fusion.1
  90.6 0.9 fusion.15
  91.5 0.1 reshape.92
  91.6 0.1 reshape.108
  91.7 0.8 fusion.23
  92.5 0.1 copy.32
  92.6 0.1 reshape.100
  92.7 0.1 multiply_reduce_fusion
  92.8 0.1 copy.34
  92.9 2.8 fusion.37
  95.7 0.2 select_reduce_fusion
  95.9 20.9 %pmax.7 = f32[16,12]{0,1:T(8,128)S(1)} all-reduce(f32[16,12]{0,1:T(8,128)S(1)} %get-tuple-element.19), channel_id=1, replica_groups=mesh['kv'=8,'tp'=4] {'kv'}, use_global_device_ids=true, to_apply=%region_7.8 | all-reduce | flops 192 | bytes 1536 | tf_op jit(solution)/shard_map/pmax | solution.py:86
  116.8 0.2 fusion.6
  117.0 0.6 fusion.35
  117.6 0.1 copy.35
  117.7 3.6 %fusion.4 = f32[16,12,1,64]{3,2,1,0:T(1,128)S(1)} fusion(bf16[16,128,12,64]{1,3,2,0:T(8,128)(2,1)} %bitcast.21, bf16[16,12,128,1]{2,0,1,3:T(8,128)(2,1)S(1)} %get-tuple-element.22), kind=kOutput, calls=%fused_computation.9 | convolution fusion | flops 3145728 | bytes 3244032 | tf_op jit(solution)/shard_map/bhp,bphe->bhe/dot_general | solution.py:23
  121.2 0.8 bitcast_multiply_fusion
  122.1 0.0 all-reduce.6.cloned.1.call-start
  122.1 68.6 %all-reduce.8.cloned.1.call-done = (f32[16,12,64]{2,1,0:T(8,128)}, f32[16,768]{1,0:T(8,128)}, f32[16,12]{0,1:T(8,128)}) async-done(((f32[16,12,64]{2,1,0:T(8,128)}, f32[16,768]{1,0:T(8,128)}, f32[16,12]{0,1:T(8,128)}), (f32[16,12,64]{2,1,0:T(8,128)}, f32[16,768]{1,0:T(8,128)}, f32[16,12]{0,1:T(8,128)})) %all-reduce.8.cloned.1.call-update) | async-done | bytes 99088 | tf_op jit(solution)/shard_map/psum | solution.py:89
  190.7 0.7 fusion.34
  191.4 0.1 copy.37
  191.5 0.1 copy.36
  191.6 0.9 fusion.16
  192.5 0.1 reshape.102
  192.6 1.0 divide_convert_fusion
  193.6 0.1 convert_element_type.52
  193.7 0.2 fusion.38
  193.9 10.3 %psum.92 = f32[16,512]{1,0:T(8,128)S(1)} all-reduce(f32[16,512]{1,0:T(8,128)S(1)} %fusion.38), channel_id=1, replica_groups=mesh['kv'=8,'tp'=4] {'tp'}, use_global_device_ids=true, to_apply=%region_14.15 | all-reduce | flops 8192 | bytes 65536 | tf_op jit(solution)/shard_map/psum | solution.py:103
  204.2 0.1 fusion.12
  204.3 3.6 %fusion.17 = f32[16,4096]{1,0:T(8,128)} fusion(bf16[512,4096]{1,0:T(8,128)(2,1)} %param.22, bf16[16,512]{1,0:T(8,128)(2,1)S(1)} %get-tuple-element.14, f32[512]{0:T(512)S(1)} %copy-done.4), kind=kOutput, calls=%fused_computation.35 | convolution fusion | flops 67133440 | bytes 4474880 | tf_op jit(solution)/shard_map/dot_general | solution.py:106
  207.9 19.7 %psum.93 = f32[16]{0:T(128)S(1)} all-reduce(f32[16]{0:T(128)S(1)} %get-tuple-element.13), channel_id=1, replica_groups=mesh['kv'=8,'tp'=4] {'kv'}, use_global_device_ids=true, to_apply=%region_16.17 | all-reduce | flops 16 | bytes 128 | tf_op jit(solution)/shard_map/psum | solution.py:108
  227.6 50.8 %all-reduce.6.cloned.1.call-done = f32[16,4096]{1,0:T(8,128)} async-done(((f32[16,4096]{1,0:T(8,128)}), f32[16,4096]{1,0:T(8,128)}) %all-reduce.6.cloned.1.call-update) | async-done | bytes 262160 | tf_op jit(solution)/shard_map/psum | solution.py:108
  278.4 3.0 fusion
  281.4 10.3 %psum.95 = f32[16,512]{1,0:T(8,128)S(1)} all-reduce(f32[16,512]{1,0:T(8,128)S(1)} %fusion), channel_id=1, replica_groups=mesh['kv'=8,'tp'=4] {'tp'}, use_global_device_ids=true, to_apply=%region_18.19 | all-reduce | flops 8192 | bytes 65536 | tf_op jit(solution)/shard_map/psum | solution.py:112
  291.6 0.6 fusion.14
  (16 shorter events, 0.1 us)
Async XLA Ops:
  6.5 4.5 %copy-start = (bf16[512,768]{1,0:T(8,128)(2,1)S(1)}, bf16[512,768]{1,0:T(8,128)(2,1)}, u32[]{:S(2)}) copy-start(bf16[512,768]{1,0:T(8,128)(2,1)} %param.16) | copy-start | bytes 2359300
  6.5 83.4 %all-reduce.10.cloned.1.call-start = ((), (), s32[]{:S(2)}) async-start(), calls=%async_computation.2 | async-start | bytes 230400 | tf_op jit(solution)/shard_map/psum | solution.py:59
  16.1 174.6 %all-reduce.8.cloned.1.call-start = ((), (), s32[]{:S(2)}) async-start(), calls=%async_computation.1 | async-start | bytes 376832 | tf_op jit(solution)/shard_map/psum | solution.py:89
  27.5 68.2 %copy-start.3 = (f32[16,12,128]{2,0,1:T(8,128)S(1)}, f32[16,12,128]{2,0,1:T(8,128)}, u32[]{:S(2)}) copy-start(f32[16,12,128]{2,0,1:T(8,128)} %param.26) | copy-start | bytes 294916
  95.7 98.0 %copy-start.1 = (bf16[768,512]{1,0:T(8,128)(2,1)S(1)}, bf16[768,512]{1,0:T(8,128)(2,1)}, u32[]{:S(2)}) copy-start(bf16[768,512]{1,0:T(8,128)(2,1)} %param.20) | copy-start | bytes 2359300
  95.7 108.5 %copy-start.2 = (bf16[16,512]{1,0:T(8,128)(2,1)S(1)}, bf16[16,512]{1,0:T(8,128)(2,1)}, u32[]{:S(2)}) copy-start(bf16[16,512]{1,0:T(8,128)(2,1)} %param.14) | copy-start | bytes 49156
  95.7 108.7 %copy-start.4 = (f32[512]{0:T(512)S(1)}, f32[512]{0:T(512)}, u32[]{:S(2)}) copy-start(f32[512]{0:T(512)} %param.21) | copy-start | bytes 6148
  122.1 156.3 %all-reduce.6.cloned.1.call-start = ((), (), s32[]{:S(2)}) async-start(), calls=%async_computation | async-start | bytes 524288 | tf_op jit(solution)/shard_map/psum | solution.py:108
Sparse Core Ops, SparseCore 0:
  16.2 73.6 all-reduce.9
  122.2 68.4 all-reduce.7
  208.0 70.3 all-reduce.5
where the time goes:
time: 300 us; the launch traced here: 299 us
  waiting for transfers between devices  182 us (61%)
  blocking collectives  61.1 us (20%)
  matrix products  20.2 us (7%)
  between operations  13.2 us (4%)
  other arithmetic  11.4 us (4%)
  local copies, waits for them, and re-layouts  10.9 us (4%)
    psum x1, waiting for transfers between devices, shards(): lax.psum((local_state[1] * factor_here, local_state[2] * factor_here[...,...  68.6 us
    psum x1, waiting for transfers between devices, shards(): lax.psum((jnp.dot(scaled_in, w_query, preferred_element_type=jnp.float32)...  62.4 us
    psum x1, waiting for transfers between devices, shards(): upward, squares_all = lax.psum((up_terms, squares_here), 'kv')  50.8 us
    pmax x1, blocking collectives, shards(): global_peak = lax.pmax(local_state[0], 'kv')  20.9 us
    psum x1, blocking collectives, shards(): upward, squares_all = lax.psum((up_terms, squares_here), 'kv')  19.7 us
    psum x1, blocking collectives, shards(): lax.psum(jnp.dot(attended, w_out, preferred_element_type=jnp.float32), 'tp')  10.3 us
    psum x1, blocking collectives, shards(): channel_terms = lax.psum(down_terms, 'tp')  10.3 us
    unnamed x12, local copies, waits for them, and re-layouts  9.35 us
  transfers between devices with their start and end apart: 3, of which 3 were waited for; matrix products, arithmetic and copies ran while one was open for 4% of the time, Pallas kernels for 0%

commit v1 on v0

--- a/solution.py
+++ b/solution.py
@@ -1,13 +1,429 @@
+import functools
+
 import jax
 import jax.numpy as jnp
 from jax import lax
+from jax.experimental import pallas as pl
+from jax.experimental.pallas import tpu as pltpu
 from jax.sharding import PartitionSpec as P
 
 HEAD_DIM = 64
-
 
 epsilon = 1e-06
 very_low = -1e30
+LANES = 128
+F32 = jnp.float32
+BF16 = jnp.bfloat16
+
+EX_Q, EX_SMALL, EX_KV, EX_O, EX_LSE, EX_OUT, EX_UP, EX_SQ, EX_HID, EX_DOWN = range(10)
+LANE_NEWEST = 32
+LANE_SQUARES = 64
+
+
+def mm(a, b):
+    return jnp.dot(a, b, preferred_element_type=F32)
+
+
+def split_mm(a, b):
+    high = a.astype(BF16)
+    low = (a - high.astype(F32)).astype(BF16)
+    return mm(high, b) + mm(low, b)
+
+
+def mm_t(a, spread):
+    return lax.dot_general(a, spread, (((1,), (1,)), ((), ())), preferred_element_type=F32)
+
+
+def layer_kernel(
+    n_kv,
+    n_tp,
+    lengths,
+    tokens_h,
+    gain_h,
+    wq_h,
+    wk_h,
+    wv_h,
+    wf_h,
+    wo_h,
+    mix_gain_h,
+    wu_h,
+    wd_h,
+    kc_h,
+    vc_h,
+    decay_h,
+    out_h,
+    tokens_v,
+    gain_v,
+    wq,
+    wk,
+    wv,
+    wf,
+    wo,
+    mix_gain_v,
+    wu,
+    wd,
+    kc,
+    vc,
+    decay,
+    q_all,
+    small_all,
+    kv_send,
+    kv_all,
+    q_s,
+    bias_s,
+    base_s,
+    now_s,
+    o_s,
+    lse_s,
+    o_all,
+    lse_all,
+    out_all,
+    up_send,
+    up_all,
+    sq_all,
+    hid_all,
+    down_all,
+    load_sem,
+    send_sem,
+    recv_sem,
+):
+    j = lax.axis_index("kv")
+    t = lax.axis_index("tp")
+    rows, feats = tokens_v.shape
+    width = feats * n_kv
+    att = wq.shape[1]
+    heads = decay.shape[0]
+    span = decay.shape[2]
+    own_rows = rows // n_kv
+    chunk = wu.shape[1] // n_kv
+
+    loads = [
+        pltpu.make_async_copy(src, dst, load_sem.at[i])
+        for i, (src, dst) in enumerate(
+            [
+                (tokens_h, tokens_v),
+                (gain_h, gain_v),
+                (wf_h, wf),
+                (wq_h, wq),
+                (decay_h, decay),
+                (wk_h, wk),
+                (wv_h, wv),
+                (kc_h, kc),
+                (vc_h, vc),
+                (wo_h, wo),
+                (mix_gain_h, mix_gain_v),
+                (wu_h, wu),
+                (wd_h, wd),
+            ]
+        )
+    ]
+    names = ("tok", "gain", "wf", "wq", "decay", "wk", "wv", "kc", "vc", "wo", "mg", "wu", "wd")
+    L = dict(zip(names, loads))
+    barrier = pltpu.get_barrier_semaphore()
+    for k in range(1, n_kv):
+        pl.semaphore_signal(
+            barrier, inc=1, device_id={"kv": lax.rem(j + k, n_kv)}, device_id_type=pl.DeviceIdType.MESH
+        )
+    for k in range(1, n_tp):
+        pl.semaphore_signal(
+            barrier, inc=1, device_id={"tp": lax.rem(t + k, n_tp)}, device_id_type=pl.DeviceIdType.MESH
+        )
+
+    for name in names[:5]:
+        L[name].start()
+
+    def copy(ex, src, dst, axis, peer, me):
+        return pltpu.make_async_remote_copy(
+            src_ref=src,
+            dst_ref=dst,
+            send_sem=send_sem.at[ex, peer],
+            recv_sem=recv_sem.at[ex, me],
+            device_id={axis: peer},
+            device_id_type=pl.DeviceIdType.MESH,
+        )
+
+    sent = []
+
+    def send(ex, src, dst, axis, peer, me):
+        c = copy(ex, src, dst, axis, peer, me)
+        c.start()
+        sent.append(c)
+
+    def arrived(ex, buf, axis, peer):
+        copy(ex, buf.at[peer], buf.at[peer], axis, peer, peer).wait_recv()
+
+    kv_peers = [lax.rem(j + k, n_kv) for k in (4, 3, 5, 2, 6, 1, 7)] if n_kv == 8 else [
+        lax.rem(j + k, n_kv) for k in range(1, n_kv)
+    ]
+    tp_peers = [lax.rem(t + k, n_tp) for k in range(1, n_tp)]
+
+    lane = lax.broadcasted_iota(jnp.int32, (heads, LANES), 1)
+    sub = lax.broadcasted_iota(jnp.int32, (heads, LANES), 0)
+    eye = lane == sub
+    eye_newest = lane == sub + LANE_NEWEST
+    head_mask = (
+        lax.broadcasted_iota(jnp.int32, (heads, att), 1) // HEAD_DIM
+        == lax.broadcasted_iota(jnp.int32, (heads, att), 0)
+    )
+    spread = (
+        lax.broadcasted_iota(jnp.int32, (LANES, att), 1) // HEAD_DIM
+        == lax.broadcasted_iota(jnp.int32, (LANES, att), 0)
+    ).astype(F32).astype(BF16)
+    position = lax.broadcasted_iota(jnp.int32, (heads, span), 1) + j * span
+    lane_r = lax.broadcasted_iota(jnp.int32, (rows, LANES), 1)
+
+    L["tok"].wait()
+    L["gain"].wait()
+    tokens_f = tokens_v[...].astype(F32)
+    scaled_in = (tokens_f * gain_v[...]).astype(BF16)
+    squares = jnp.sum(tokens_f * tokens_f, axis=1, keepdims=True)
+    L["wf"].wait()
+    forget = mm_t(scaled_in, wf[...])
+    mine = forget[:, 0:heads]
+    for k in range(1, n_tp):
+        mine = jnp.where(t == k, forget[:, k * heads : (k + 1) * heads], mine)
+    L["wq"].wait()
+    for name in names[5:]:
+        L[name].start()
+    q_all[j] = mm(scaled_in, wq[...]).astype(BF16)
+    L["decay"].wait()
+    for b in range(rows):
+        fall = decay[:, b, :]
+        hit = jnp.sum(jnp.where(position == lengths[b] - 1, fall, 0.0), axis=1, keepdims=True)
+        now_s[b : b + 1, :] = jnp.sum(jnp.where(eye_newest, hit, 0.0), axis=0, keepdims=True)
+    small_all[j] = now_s[...] + jnp.where(lane_r == LANE_SQUARES, squares, 0.0)
+    small_all[j, :, 0:heads] = mine
+
+    pl.semaphore_wait(barrier, n_kv - 1 + n_tp - 1)
+    for d in kv_peers:
+        send(EX_Q, q_all.at[j], q_all.at[j], "kv", d, j)
+        send(EX_SMALL, small_all.at[j], small_all.at[j], "kv", d, j)
+    L["wk"].wait()
+    new_k = mm(scaled_in, wk[...])
+    L["wv"].wait()
+    new_v = mm(scaled_in, wv[...])
+    for d in range(n_kv):
+        kv_send[d, :, 0:att] = new_k[d * own_rows : (d + 1) * own_rows].astype(BF16)
+        kv_send[d, :, att:] = new_v[d * own_rows : (d + 1) * own_rows].astype(BF16)
+    kv_all[j] = kv_send[j]
+    for d in kv_peers:
+        send(EX_KV, kv_send.at[d], kv_all.at[j], "kv", d, j)
+
+    for b in range(rows):
+        fall = decay[:, b, :]
+        base = fall[:, 0:1]
+        bias_s[b] = jnp.where(position < lengths[b], base - fall, very_low)
+        base_s[b : b + 1, :] = jnp.sum(jnp.where(eye, base, 0.0), axis=0, keepdims=True)
+
+    for d in reversed(kv_peers):
+        arrived(EX_SMALL, small_all, "kv", d)
+        arrived(EX_Q, q_all, "kv", d)
+    small = jnp.sum(small_all[...], axis=0)
+    row_scale = lax.rsqrt(small[:, LANE_SQUARES : LANE_SQUARES + 1] / width + epsilon)
+    gate = row_scale * small[:, 0:heads]
+    log_forget = jnp.minimum(gate, 0.0) - jnp.log1p(jnp.exp(-jnp.abs(gate)))
+    now_s[...] = jnp.zeros_like(now_s)
+    now_s[:, 0:heads] = small[:, LANE_NEWEST : LANE_NEWEST + heads] + log_forget
+    q_sum = q_all[0].astype(F32)
+    for d in range(1, n_kv):
+        q_sum += q_all[d].astype(F32)
+    q_s[...] = (row_scale * q_sum).astype(BF16).astype(F32)
+
+    L["kc"].wait()
+    scores = []
+    for b in range(rows):
+        query = jnp.where(head_mask, q_s[b : b + 1, :], 0.0).astype(BF16)
+        scores.append(mm_t(query, kc[b]))
+    weights = []
+    inverse = []
+    for b in range(rows):
+        live = position < lengths[b]
+        s = jnp.where(live, scores[b] * HEAD_DIM ** (-0.5) + bias_s[b], very_low)
+        peak = jnp.max(s, axis=1, keepdims=True)
+        w = jnp.where(live, jnp.exp(s - peak), 0.0)
+        total = jnp.sum(w, axis=1, keepdims=True)
+        some = total > 0.0
+        safe = jnp.where(some, total, 1.0)
+        weights.append(w.astype(BF16))
+        inverse.append(1.0 / safe)
+        lse = jnp.where(some, peak + jnp.log(safe), very_low)
+        lse_s[b : b + 1, :] = jnp.sum(jnp.where(eye, lse, 0.0), axis=0, keepdims=True)
+    L["vc"].wait()
+    for b in range(rows):
+        part = mm(weights[b], vc[b]) * inverse[b]
+        o_s[b : b + 1, :] = jnp.sum(jnp.where(head_mask, part, 0.0), axis=0, keepdims=True)
+    lse_s[...] = jnp.where(lse_s[...] > very_low, lse_s[...] + (now_s[...] - base_s[...]), very_low)
+
+    for d in reversed(kv_peers):
+        arrived(EX_KV, kv_all, "kv", d)
+    kv_here = jnp.sum(kv_all[...].astype(F32), axis=0)
+    row_kv = lax.broadcasted_iota(jnp.int32, (rows, 2 * att), 0)
+    kv_sum = jnp.zeros((rows, 2 * att), F32)
+    for r in range(own_rows):
+        kv_sum = jnp.where(row_kv == j * own_rows + r, kv_here[r : r + 1, :], kv_sum)
+    kv_new = (row_scale * kv_sum).astype(BF16).astype(F32)
+    product = q_s[...] * kv_new[:, 0:att]
+    high = product.astype(BF16)
+    low = (product - high.astype(F32)).astype(BF16)
+    own_score = HEAD_DIM ** (-0.5) * (mm_t(high, spread) + mm_t(low, spread))
+    owned = lax.broadcasted_iota(jnp.int32, (rows, LANES), 0) // own_rows == j
+    own_score = jnp.where(owned, own_score, very_low)
+    lse_old = lse_s[...]
+    top = jnp.maximum(lse_old, own_score)
+    part_old = jnp.where(lse_old > very_low, jnp.exp(lse_old - top), 0.0)
+    part_new = jnp.where(owned, jnp.exp(own_score - top), 0.0)
+    both = part_old + part_new
+    some = both > 0.0
+    both = jnp.where(some, both, 1.0)
+    lse_all[j] = jnp.where(some, top + jnp.log(both), very_low)
+    o_all[j] = (
+        split_mm(part_old / both, spread) * o_s[...]
+        + split_mm(part_new / both, spread) * kv_new[:, att:]
+    ).astype(BF16)
+    for d in kv_peers:
+        send(EX_LSE, lse_all.at[j], lse_all.at[j], "kv", d, j)
+        send(EX_O, o_all.at[j], o_all.at[j], "kv", d, j)
+    for d in reversed(kv_peers):
+        arrived(EX_LSE, lse_all, "kv", d)
+    lse = lse_all[...]
+    share = jnp.exp(lse - jnp.max(lse, axis=0, keepdims=True))
+    share = share / jnp.sum(share, axis=0, keepdims=True)
+    shares = split_mm(share.reshape(n_kv * rows, LANES), spread)
+    for d in reversed(kv_peers):
+        arrived(EX_O, o_all, "kv", d)
+    attended = shares[0:rows] * o_all[0].astype(F32)
+    for d in range(1, n_kv):
+        attended += shares[d * rows : (d + 1) * rows] * o_all[d].astype(F32)
+    attended = attended.astype(BF16)
+
+    L["wo"].wait()
+    out_all[t] = mm(attended, wo[...]).astype(BF16)
+    for d in tp_peers:
+        send(EX_OUT, out_all.at[t], out_all.at[t], "tp", d, t)
+    for d in tp_peers:
+        arrived(EX_OUT, out_all, "tp", d)
+    head_terms = out_all[0].astype(F32)
+    for d in range(1, n_tp):
+        head_terms += out_all[d].astype(F32)
+    mixed = (tokens_f + head_terms).astype(BF16).astype(F32)
+
+    L["mg"].wait()
+    mix_in = (mixed * mix_gain_v[...]).astype(BF16)
+    sq_all[j] = jnp.broadcast_to(jnp.sum(mixed * mixed, axis=1, keepdims=True), (rows, LANES))
+    for d in kv_peers:
+        send(EX_SQ, sq_all.at[j], sq_all.at[j], "kv", d, j)
+    L["wu"].wait()
+    for d in kv_peers:
+        up_send[d] = mm(mix_in, wu[:, pl.ds(pl.multiple_of(d * chunk, chunk), chunk)]).astype(BF16)
+        send(EX_UP, up_send.at[d], up_all.at[j], "kv", d, j)
+    up_all[j] = mm(mix_in, wu[:, pl.ds(pl.multiple_of(j * chunk, chunk), chunk)]).astype(BF16)
+    for d in reversed(kv_peers):
+        arrived(EX_SQ, sq_all, "kv", d)
+    mix_scale = lax.rsqrt(jnp.sum(sq_all[...], axis=0)[:, 0:1] / width + epsilon)
+    for d in reversed(kv_peers):
+        arrived(EX_UP, up_all, "kv", d)
+    upward = up_all[0].astype(F32)
+    for d in range(1, n_kv):
+        upward += up_all[d].astype(F32)
+    act = jnp.maximum(mix_scale * upward, 0.0)
+    hid_all[j] = (act * act).astype(BF16)
+    for d in kv_peers:
+        send(EX_HID, hid_all.at[j], hid_all.at[j], "kv", d, j)
+    L["wd"].wait()
+
+    def down(d):
+        return mm(hid_all[d], wd[pl.ds(pl.multiple_of(d * chunk, chunk), chunk), :])
+
+    total = down(j)
+    for d in reversed(kv_peers):
+        arrived(EX_HID, hid_all, "kv", d)
+        total += down(d)
+    down_all[t] = total.astype(BF16)
+    for d in tp_peers:
+        send(EX_DOWN, down_all.at[t], down_all.at[t], "tp", d, t)
+    for d in tp_peers:
+        arrived(EX_DOWN, down_all, "tp", d)
+    channel = down_all[0].astype(F32)
+    for d in range(1, n_tp):
+        channel += down_all[d].astype(F32)
+    out_h[...] = (mixed + channel).astype(BF16)
+    for c in sent:
+        c.wait_send()
+
+
+def fast_shards(
+    n_kv,
+    n_tp,
+    tokens,
+    norm_gain,
+    w_query,
+    w_key,
+    w_value,
+    w_forget,
+    w_out,
+    mix_gain,
+    w_up,
+    w_down,
+    key_cache,
+    value_cache,
+    decay_cache,
+    lengths,
+):
+    rows, feats = tokens.shape
+    att = w_query.shape[1]
+    own_rows = rows // n_kv
+    chunk = w_up.shape[1] // n_kv
+    operands = (
+        tokens,
+        norm_gain.reshape(1, feats),
+        w_query,
+        w_key,
+        w_value,
+        w_forget.T,
+        w_out,
+        mix_gain.reshape(1, feats),
+        w_up,
+        w_down,
+        key_cache,
+        value_cache,
+        decay_cache.transpose(1, 0, 2),
+    )
+    big = max(n_kv, n_tp)
+    span = decay_cache.shape[2]
+    scratch = [pltpu.VMEM(a.shape, a.dtype) for a in operands] + [
+        pltpu.VMEM((n_kv, rows, att), BF16),
+        pltpu.VMEM((n_kv, rows, LANES), F32),
+        pltpu.VMEM((n_kv, own_rows, 2 * att), BF16),
+        pltpu.VMEM((n_kv, own_rows, 2 * att), BF16),
+        pltpu.VMEM((rows, att), F32),
+        pltpu.VMEM((rows, decay_cache.shape[1], span), F32),
+        pltpu.VMEM((rows, LANES), F32),
+        pltpu.VMEM((rows, LANES), F32),
+        pltpu.VMEM((rows, att), F32),
+        pltpu.VMEM((rows, LANES), F32),
+        pltpu.VMEM((n_kv, rows, att), BF16),
+        pltpu.VMEM((n_kv, rows, LANES), F32),
+        pltpu.VMEM((n_tp, rows, feats), BF16),
+        pltpu.VMEM((n_kv, rows, chunk), BF16),
+        pltpu.VMEM((n_kv, rows, chunk), BF16),
+        pltpu.VMEM((n_kv, rows, LANES), F32),
+        pltpu.VMEM((n_kv, rows, chunk), BF16),
+        pltpu.VMEM((n_tp, rows, feats), BF16),
+        pltpu.SemaphoreType.DMA((len(operands),)),
+        pltpu.SemaphoreType.DMA((10, big)),
+        pltpu.SemaphoreType.DMA((10, big)),
+    ]
+    return pl.pallas_call(
+        functools.partial(layer_kernel, n_kv, n_tp),
+        out_shape=jax.ShapeDtypeStruct(tokens.shape, tokens.dtype),
+        in_specs=[pl.BlockSpec(memory_space=pltpu.SMEM)]
+        + [pl.BlockSpec(memory_space=pl.ANY)] * len(operands),
+        out_specs=pl.BlockSpec(memory_space=pltpu.VMEM),
+        scratch_shapes=scratch,
+        compiler_params=pltpu.CompilerParams(
+            collective_id=0, has_side_effects=True, vmem_limit_bytes=56 * 1024 * 1024
+        ),
+    )(lengths, *operands)
 
 
 def local_softmax(query_heads, score_bias, keys_block, values_block, live_mask):
@@ -113,6 +529,19 @@
     return (mixed_f + channel_terms).astype(jnp.bfloat16)
 
 
+def fits(n_kv, *operands):
+    tokens, w_query, w_up, decay = (operands[0], operands[2], operands[8], operands[12])
+    rows, feats = tokens.shape
+    return (
+        rows % n_kv == 0
+        and feats % LANES == 0
+        and w_query.shape[1] % LANES == 0
+        and w_up.shape[1] % (n_kv * LANES) == 0
+        and decay.shape[2] % LANES == 0
+        and decay.shape[1] <= LANE_NEWEST
+    )
+
+
 def solution(mesh):
     placed = (
         P(None, "kv"),
@@ -130,6 +559,12 @@
         P(None, "tp", "kv"),
         P(),
     )
+    n_kv, n_tp = mesh.shape["kv"], mesh.shape["tp"]
+
+    def layer(*operands):
+        body = functools.partial(fast_shards, n_kv, n_tp) if fits(n_kv, *operands) else shards
+        return body(*operands)
+
     return jax.shard_map(
-        shards, mesh=mesh, in_specs=placed, out_specs=P(None, "kv"), check_vma=False
-    )
+        layer, mesh=mesh, in_specs=placed, out_specs=P(None, "kv"), check_vma=False
+    )

time: 300 us -> 45 us (0.15)
  waiting for transfers between devices: 182 us -> 0 us
  blocking collectives: 61.1 us -> 0 us
  Pallas kernels: 0 us -> 43.3 us
  matrix products: 20.2 us -> 0 us
  between operations: 13.2 us -> 0.01 us
  other arithmetic: 11.4 us -> 0 us
  local copies, waits for them, and re-layouts: 10.9 us -> 1.32 us
    psum x3 -> x0, waiting for transfers between devices: 182 us -> none  [the longest x1 68.6 us: shards(): lax.psum((local_state[1] * factor_here, local_state[2] * factor_here[...,...]
    pallas_call x0 -> x1, Pallas kernels: none -> 43.3 us  [fast_shards(): pl.pallas_call(functools.partial(layer_kernel, n_kv, n_tp), out_shape=jax...]
    psum x3 -> x0, blocking collectives: 40.2 us -> none  [the longest x1 19.7 us: shards(): upward, squares_all = lax.psum((up_terms, squares_here), 'kv')]
    pmax x1 -> x0, blocking collectives: 20.9 us -> none  [shards(): global_peak = lax.pmax(local_state[0], 'kv')]
    dot_general x9 -> x0, matrix products: 20.2 us -> none  [the longest x1 3.6 us: local_softmax(): jnp.einsum('bhp,bphe->bhe', weights.astype(jnp.bfloat16), values_view, pr...]
    unnamed x12 -> x1, local copies, waits for them, and re-layouts: 9.35 us -> 1.32 us
  transfers between devices with their start and end apart: 3 -> 0, of which waited for: 3 -> 0; matrix products, arithmetic and copies ran while one was open for 4% -> 0% of each run, Pallas kernels for 0% -> 0%
where the time goes in v1:
time: 45 us; the launch traced here: 44.6 us
  Pallas kernels  43.3 us (96%)
  local copies, waits for them, and re-layouts  1.32 us (3%)
    pallas_call x1, Pallas kernels, fast_shards(): pl.pallas_call(functools.partial(layer_kernel, n_kv, n_tp), out_shape=jax...  43.3 us
    unnamed x1, local copies, waits for them, and re-layouts  1.32 us

profile of v1, /device:TPU:0, one launch (start us, length us, event | category | flops | bytes accessed | tf_op | source)
XLA Modules:
  0.0 44.6 jit_solution(2809224195034261456)
XLA Ops:
  0.0 43.3 %shard_map.136 = bf16[16,512]{1,0:T(8,128)(2,1)} custom-call(s32[16]{0:T(128)} %lengths.1, bf16[16,512]{1,0:T(8,128)(2,1)} %tokens_h.1, f32[1,512]{1,0:T(1,128)} %bitcast.6, bf16[512,768]{1,0:T(8,128)(2,1)} %wq_h.1, bf16[512,768]{1,0:T(8,128)(2,1)} %wk_h.1, bf16[512,768]{1,0:T(8,128)(2,1)} %wv_h.1, bf16[48,512]{1,0:T(8,128)(2,1)} %bitcast.5, ...), custom_call_target="tpu_custom_call" | custom-call | tf_op jit(solution)/shard_map/pallas_call | solution.py:416
  43.3 1.3 %copy.16 = bf16[16,512]{1,0:T(8,128)(2,1)} copy(bf16[16,512]{1,0:T(8,128)(2,1)} %shard_map.136) | data formatting | bytes 32768
